TPU v7x, 32 devices: a whole 2x2x4 slice. The times are simulated.
32 devices in a mesh: grp: 2 (over y), ep: 4 (over z), tp: 4 (over x, core).
Axes of the slice: x: 2, y: 2, z: 4, core: 2. Of those that a mesh axis runs over, the one named last changes fastest.
Arguments:
- queries: bfloat16 [1024, 1024], P(('grp', 'ep'), 'tp'), parts along dimension 0, may hold values from -6 to 6
- keys: bfloat16 [1024, 1024], P(('grp', 'ep'), 'tp'), parts along dimension 0, may hold values from -6 to 6
- values: bfloat16 [1024, 1024], P(('grp', 'ep'), 'tp'), parts along dimension 0, may hold values from -6 to 6
- lambdas: float32 [8], P('tp'), may hold values from 0.3 to 0.8
- head_gain: float32 [128], replicated, may hold values from 0.1 to 1.9
- tokens: bfloat16 [2048, 1536], P(('grp', 'ep')), parts along dimension 0, may hold values from -6 to 6
- route_ids: int32 [2048, 2], P(('grp', 'ep')), parts along dimension 0, may hold values from 0 to 3, all different within a row; in each aligned block of 256 rows (0 to 255, 256 to 511, ...) at most 256 rows name the same one
- route_weights: float32 [2048, 2], P(('grp', 'ep')), parts along dimension 0, may hold values from 0.2 to 1
- moe_gain: float32 [1536], replicated, may hold values from 0.1 to 1.9
- w_gate: bfloat16 [4, 1536, 3072], P('ep', None, 'tp'), may hold values from -0.15625 to 0.15625
- w_up: bfloat16 [4, 1536, 3072], P('ep', None, 'tp'), may hold values from -0.15625 to 0.15625
- w_down: bfloat16 [4, 3072, 1536], P('ep', 'tp'), may hold values from -0.109375 to 0.109375
Outputs:
- heads_out: bfloat16 [1024, 1024], P(('grp', 'ep'), 'tp'), parts along dimension 0
- expert_out: bfloat16 [2048, 1536], P(('grp', 'ep'), 'tp'), parts along dimension 0
There are 2 independent parts, one for each index of `grp`. A program takes and returns all parts, laid end to end along the dimension named above; an argument that names none is the same for every part. Nothing has to cross between parts.
Inputs may be any that keep to these rules, and one draw needn't show every extreme that they name: `route_ids`: each row names 2 different experts. In the 256 rows of one device no expert is named more than 256 times, and in every draw some device names some expert exactly 256 times.
All inputs are finite; a program needn't handle non-finite values.
Results may differ from a plain program's by a relative error of at most 0.015.
Values may be sent and summed in bfloat16 or wider, within the bound.
A program may use at most 64 MiB of HBM per device.

v0:
```python
import functools

import jax
import jax.numpy as jnp
from jax import lax
from jax.experimental import pallas as pl
from jax.experimental.pallas import tpu as pltpu
from jax.sharding import PartitionSpec as P

MESH = pl.DeviceIdType.MESH
F32 = jnp.float32
BF16 = jnp.bfloat16
PIECES = 2

def attend(queries, keys, values, lambdas, head_gain):
    row_count = queries.shape[0]
    head_count = lambdas.shape[0]
    head_dim = queries.shape[1] // (2 * head_count)
    value_dim = values.shape[1] // head_count
    query_parts = queries.reshape(row_count, head_count, 2, head_dim)
    score_scale = head_dim ** (-0.5)
    running = jnp.full((head_count, 2, row_count), -1e30, jnp.float32)
    key_piece = lax.all_gather(keys, "ep", axis=0, tiled=True)
    value_piece = lax.all_gather(values, "ep", axis=0, tiled=True)
    count = key_piece.shape[0]
    key_parts = key_piece.reshape(count, head_count, 2, head_dim)
    value_parts = value_piece.reshape(count, head_count, value_dim)
    scores = (
        jnp.einsum("qhcd,khcd->hcqk", query_parts, key_parts, preferred_element_type=jnp.float32)
        * score_scale
    )
    newest = jnp.maximum(running, jnp.max(scores, axis=-1))
    weights_now = jnp.exp(scores - newest[..., None])
    totals = jnp.sum(weights_now, axis=-1)
    sums = jnp.einsum(
        "hcqk,khe->hcqe",
        weights_now.astype(jnp.bfloat16),
        value_parts,
        preferred_element_type=jnp.float32,
    )
    running, totals, sums = (newest, totals, sums)
    means = sums / totals[..., None]
    mixed = means[:, 0] - lambdas[:, None, None] * means[:, 1]
    scaled = mixed * lax.rsqrt(jnp.mean(mixed * mixed, axis=-1, keepdims=True) + 1e-06) * head_gain
    return (
        jnp.transpose(scaled, (1, 0, 2))
        .reshape(row_count, head_count * value_dim)
        .astype(jnp.bfloat16)
    )


def experts(tokens, route_ids, route_weights, moe_gain, w_gate, w_up, w_down):
    row_count, width = tokens.shape
    top_count = route_ids.shape[1]
    ep_size = lax.axis_size("ep")
    tp_size = lax.axis_size("tp")
    expert_count = w_gate.shape[0] * ep_size
    capacity = 2 * row_count * top_count // expert_count
    token_float = tokens.astype(jnp.float32)
    normed = (
        token_float
        * lax.rsqrt(jnp.mean(token_float * token_float, axis=1, keepdims=True) + 1e-06)
        * moe_gain
    ).astype(jnp.bfloat16)
    flat_ids = route_ids.reshape(-1)
    onehot = (flat_ids[:, None] == jnp.arange(expert_count, dtype=jnp.int32)[None, :]).astype(
        jnp.int32
    )
    earlier = jnp.cumsum(onehot, axis=0) - onehot
    position = jnp.sum(earlier * onehot, axis=1)
    slot_index = flat_ids * capacity + position
    owners = (
        jnp.full((expert_count * capacity,), row_count, jnp.int32)
        .at[slot_index]
        .set(jnp.arange(row_count * top_count, dtype=jnp.int32) // top_count)
    )
    padded = jnp.concatenate([normed, jnp.zeros((1, width), jnp.bfloat16)], axis=0)
    outgoing = padded[owners].reshape(expert_count, capacity, width)
    gate_mat = w_gate[0]
    up_mat = w_up[0]
    down_mat = w_down[0]
    slice_width = width // tp_size
    own_columns = lax.dynamic_slice_in_dim(
        outgoing, lax.axis_index("tp") * slice_width, slice_width, 2
    )
    arrived = lax.all_to_all(own_columns, "ep", split_axis=0, concat_axis=0, tiled=True)
    piece = lax.all_gather(arrived, "tp", axis=2, tiled=True)
    gate = jnp.einsum("scd,df->scf", piece, gate_mat, preferred_element_type=jnp.float32)
    upward = jnp.einsum("scd,df->scf", piece, up_mat, preferred_element_type=jnp.float32)
    hidden = (jax.nn.silu(gate) * upward).astype(jnp.bfloat16)
    flat_hidden = hidden.reshape(-1, hidden.shape[2])
    summed = lax.psum_scatter(
        jnp.einsum("fd,sf->ds", down_mat, flat_hidden, preferred_element_type=jnp.float32).astype(
            jnp.bfloat16
        ),
        "tp",
        scatter_dimension=0,
        tiled=True,
    )
    back = lax.all_to_all(summed, "ep", split_axis=1, concat_axis=1, tiled=True)
    picked = (
        jnp.take(back, slot_index, axis=1).astype(jnp.float32).reshape(-1, row_count, top_count)
    )
    combined = jnp.einsum("drk,rk->rd", picked, route_weights)
    return combined.astype(jnp.bfloat16)


def visit_order(n):
    return [sorted((s for s in range(n) if s != e), key=lambda s: (abs(s - e), s)) for e in range(n)]


def fused_kernel(
    n,
    q_ref,
    k_ref,
    v_ref,
    lam_ref,
    hgain_ref,
    tok_ref,
    ids_ref,
    rw_ref,
    mgain_ref,
    wg_hbm,
    wu_hbm,
    wd_hbm,
    heads_ref,
    out_ref,
    wg,
    wu,
    wd,
    gathered,
    kbuf,
    vbuf,
    hid,
    part,
    core_in,
    s_own,
    s_out,
    x_in,
    t_out,
    ret,
    out_weights,
    wsem,
    own_send,
    z_send,
    z_recv,
    x_send,
    x_recv,
    c_send,
    c_recv,
    kv_send,
    kv_recv,
    r1_send,
    r1_recv,
    r2_send,
    r2_recv,
    r3_send,
    r3_recv,
):
    e = lax.axis_index("ep")
    t = lax.axis_index("tp")
    xi = t // 2
    ci = lax.rem(t, 2)
    core_peer = {"tp": 2 * xi + 1 - ci}
    x_peer = {"tp": 2 * (1 - xi) + ci}
    rows, width = tok_ref.shape
    cols = width // 4
    kv_rows = k_ref.shape[0]

    def colblock(j):
        return pl.ds(pl.multiple_of(j * cols, 128), cols)

    def remote(src, dst, ss, rs, dev):
        return pltpu.make_async_remote_copy(
            src_ref=src, dst_ref=dst, send_sem=ss, recv_sem=rs, device_id=dev, device_id_type=MESH
        )

    weights = [
        pltpu.make_async_copy(a, b, wsem.at[i])
        for i, (a, b) in enumerate(((wg_hbm.at[0], wg), (wu_hbm.at[0], wu), (wd_hbm.at[0], wd)))
    ]
    for c in weights:
        c.start()

    barrier = pltpu.get_barrier_semaphore()
    for d in range(1, n):
        pl.semaphore_signal(barrier, inc=1, device_id={"ep": lax.rem(e + d, n)}, device_id_type=MESH)
    pl.semaphore_signal(barrier, inc=1, device_id=core_peer, device_id_type=MESH)
    pl.semaphore_signal(barrier, inc=1, device_id=x_peer, device_id_type=MESH)

    halves = range(PIECES)
    hr = rows // PIECES

    def half(h):
        return pl.ds(h * hr, hr)

    def normalize(h):
        step = 32

        @pl.loop(0, hr // step)
        def _(i):
            sl = pl.ds(pl.multiple_of(h * hr + i * step, step), step)
            v = tok_ref[sl, :].astype(F32)
            scale = lax.rsqrt(jnp.mean(v * v, axis=1, keepdims=True) + 1e-06)
            gathered[e, sl, :] = (v * scale * mgain_ref[...]).astype(BF16)

    has_left = e > 0
    has_right = e < n - 1
    sides = ((0, has_left, e - 1), (1, has_right, e + 1))
    own_kv = pl.ds(pl.multiple_of(e * kv_rows, kv_rows), kv_rows)

    def own_tok(side, peer, h):
        blk = gathered.at[e, half(h), colblock(t)]
        return remote(blk, blk, own_send.at[side, h], z_recv.at[e, h], {"ep": peer})

    def kv_copies(s):
        dev = {"ep": s}
        return (
            remote(k_ref, kbuf.at[own_kv], kv_send.at[0, s], kv_recv.at[0, e], dev),
            remote(v_ref, vbuf.at[own_kv], kv_send.at[1, s], kv_recv.at[1, e], dev),
        )

    def kv_arrivals(s):
        sl = pl.ds(pl.multiple_of(s * kv_rows, kv_rows), kv_rows)
        return (
            remote(k_ref, kbuf.at[sl], kv_send.at[0, s], kv_recv.at[0, s], {"ep": s}),
            remote(v_ref, vbuf.at[sl], kv_send.at[1, s], kv_recv.at[1, s], {"ep": s}),
        )

    orders = visit_order(n)

    def nth(k):
        s = jnp.int32(orders[0][k])
        for i in range(1, n):
            s = jnp.where(e == i, jnp.int32(orders[i][k]), s)
        return s

    visits = [nth(k) for k in range(n - 1)]

    def forward_of(s):
        from_left = s < e
        has = jnp.logical_or(
            jnp.logical_and(from_left, has_right),
            jnp.logical_and(jnp.logical_not(from_left), has_left),
        )
        return has, {"ep": jnp.clip(jnp.where(from_left, e + 1, e - 1), 0, n - 1)}

    def z_copy(s, h):
        blk = gathered.at[s, half(h), colblock(t)]
        return remote(blk, blk, z_send.at[s, h], z_recv.at[s, h], forward_of(s)[1])

    def x_copy(s, h):
        blk = gathered.at[s, half(h), colblock(t)]
        return remote(blk, blk, x_send.at[s, h], x_recv.at[s, h], x_peer)

    def c_copy(s, h, which):
        blk = gathered.at[s, half(h), colblock(t if which == 0 else 2 * (1 - xi) + ci)]
        return remote(blk, blk, c_send.at[which, s, h], c_recv.at[which, s, h], core_peer)

    def r1_copy(s, h, xx):
        return remote(
            part.at[s, half(h), colblock(2 * xx + 1 - ci)],
            core_in.at[s, xx, half(h)],
            r1_send.at[xx, s, h],
            r1_recv.at[xx, s, h],
            core_peer,
        )

    def r2_copy(s, h):
        return remote(
            s_out.at[s, half(h)], x_in.at[s, half(h)], r2_send.at[s, h], r2_recv.at[s, h], x_peer
        )

    def r3_copy(s, h):
        return remote(
            t_out.at[s, half(h)],
            ret.at[e, half(h)],
            r3_send.at[s, h],
            r3_recv.at[e, h],
            {"ep": s},
        )

    ff = wg.shape[1]
    nb = ff // 3

    def up_step(s, b):
        sl = pl.ds(b * nb, nb)
        g = jnp.dot(gathered[s], wg[:, sl], preferred_element_type=F32)
        u = jnp.dot(gathered[s], wu[:, sl], preferred_element_type=F32)
        hid[:, sl] = (g / (1.0 + jnp.exp(-g)) * u).astype(BF16)

    def down_step(s, j):
        sl = colblock(j)
        part[s, :, sl] = jnp.dot(hid[...], wd[:, sl], preferred_element_type=F32).astype(BF16)

    def down(s):
        for xx in (1 - xi, xi):
            down_step(s, 2 * xx + 1 - ci)
            for h in halves:
                r1_copy(s, h, xx).start()
        for xx in (1 - xi, xi):
            down_step(s, 2 * xx + ci)

    def reduce_core(s):
        for h in halves:
            r1_copy(s, h, 1 - xi).wait_recv()
            s_out[s, half(h)] = (
                part[s, half(h), colblock(2 * (1 - xi) + ci)].astype(F32)
                + core_in[s, 1 - xi, half(h)].astype(F32)
            ).astype(BF16)
            r2_copy(s, h).start()
        for h in halves:
            r1_copy(s, h, xi).wait_recv()
        s_own[s] = part[s, :, colblock(t)].astype(F32) + core_in[s, xi].astype(F32)

    def reduce_x(s, send=True):
        for h in halves:
            r2_copy(s, h).wait_recv()
            t_out[s, half(h)] = (s_own[s, half(h)] + x_in[s, half(h)].astype(F32)).astype(BF16)
            if send:
                r3_copy(s, h).start()

    def take(s, h):
        z_copy(s, h).wait_recv()

        @pl.when(forward_of(s)[0])
        def _():
            z_copy(s, h).start()

    def share(s, h):
        x_copy(s, h).start()
        c_copy(s, h, 0).start()

    def arrive(s, h):
        take(s, h)
        share(s, h)

    def cross(s, h):
        x_copy(s, h).wait_recv()
        c_copy(s, h, 1).start()

    def ready(s):
        for h in halves:
            c_copy(s, h, 0).wait_recv()
            c_copy(s, h, 1).wait_recv()

    def attend(h):
        heads = lam_ref.shape[0]
        vd = v_ref.shape[1] // heads
        hd = q_ref.shape[1] // (2 * heads)
        qr = q_ref.shape[0]
        first = lax.broadcasted_iota(jnp.int32, (qr, 2 * hd), 1) < hd
        q = q_ref[:, h * 2 * hd : (h + 1) * 2 * hd].astype(F32)
        both = jnp.concatenate(
            [jnp.where(first, q, 0.0).astype(BF16), jnp.where(first, 0.0, q).astype(BF16)], axis=0
        )
        kh = kbuf[:, h * 2 * hd : (h + 1) * 2 * hd]
        vh = vbuf[:, h * vd : (h + 1) * vd]
        scores = lax.dot_general(
            both, kh, (((1,), (1,)), ((), ())), preferred_element_type=F32
        ) * (hd ** (-0.5))
        ex = jnp.exp(scores - jnp.max(scores, axis=1, keepdims=True))
        tot = jnp.sum(ex, axis=1, keepdims=True)
        sums = jnp.dot(ex.astype(BF16), vh, preferred_element_type=F32) / tot
        mixed = sums[:qr] - lam_ref[h] * sums[qr:]
        norm = lax.rsqrt(jnp.mean(mixed * mixed, axis=1, keepdims=True) + 1e-06)
        heads_ref[:, h * vd : (h + 1) * vd] = (mixed * norm * hgain_ref[...]).astype(BF16)

    for h in halves:
        normalize(h)
        if h == 0:
            pl.semaphore_wait(barrier, n + 1)
        for side, has, peer in sides:

            @pl.when(has)
            def _():
                own_tok(side, peer, h).start()

    kbuf[own_kv, :] = k_ref[...]
    vbuf[own_kv, :] = v_ref[...]

    def send_kv():
        for s in visits:
            for c in kv_copies(s):
                c.start()

    ids = ids_ref[...]
    rw = rw_ref[...]
    lines = [jnp.sum(jnp.where(ids == x, rw, 0.0), axis=0, keepdims=True) for x in [e] + visits]
    pad = (-len(lines)) % 8
    lines.append(jnp.zeros((pad, rows), F32))
    out_weights[...] = jnp.concatenate(lines, axis=0).T

    last = len(visits) - 1
    for c in weights:
        c.wait()
    for b in range(3):
        up_step(e, b)
    down(e)
    inner = jnp.logical_and(has_left, has_right)
    outer = jnp.logical_not(inner)

    @pl.when(inner)
    def _():
        for h in halves:
            arrive(visits[0], h)
            if last >= 1:
                take(visits[1], h)
        if last >= 1:
            for h in halves:
                share(visits[1], h)
        for h in halves:
            cross(visits[0], h)
        if last >= 2:
            for h in halves:
                arrive(visits[2], h)

    @pl.when(outer)
    def _():
        for h in halves:
            arrive(visits[0], h)
        for h in halves:
            cross(visits[0], h)
            if last >= 1:
                arrive(visits[1], h)

    ready(visits[0])
    for k, s in enumerate(visits):
        ahead = visits[k + 1] if k < last else None
        further = visits[k + 2] if k + 1 < last else None
        before = visits[k - 1] if k > 0 else None
        for b, group in enumerate((halves[: PIECES // 2], halves[PIECES // 2 :])):
            up_step(s, b)
            for h in group:
                if ahead is not None:
                    cross(ahead, h)
                if further is not None:
                    if k == 0:

                        @pl.when(outer)
                        def _():
                            arrive(further, h)

                    else:
                        arrive(further, h)
        if k == max(last - 2, 0):
            send_kv()
        if before is not None:
            reduce_core(before)
        up_step(s, 2)
        down(s)
        if ahead is not None:
            ready(ahead)
    for k in range(max(last - 1, 0)):
        reduce_x(visits[k])
    reduce_core(visits[last])
    reduce_core(e)
    heads = lam_ref.shape[0]
    for s in visits:
        for c in kv_arrivals(s):
            c.wait_recv()
    attend(0)
    if last >= 1:
        reduce_x(visits[last - 1])
    for h in range(1, heads):
        attend(h)
    reduce_x(visits[last])
    reduce_x(e, send=False)

    total = out_weights[:, 0:1] * t_out[e].astype(F32)
    for k, s in enumerate(visits):
        for h in halves:
            remote(
                t_out.at[s, half(h)],
                ret.at[s, half(h)],
                r3_send.at[s, h],
                r3_recv.at[s, h],
                {"ep": s},
            ).wait_recv()
        total = total + ret[s].astype(F32) * out_weights[:, k + 1 : k + 2]
    out_ref[...] = total.astype(BF16)

    for side, has, peer in sides:

        @pl.when(has)
        def _():
            for h in halves:
                own_tok(side, peer, h).wait_send()

    for s in [e] + visits:
        for h in halves:
            r1_copy(s, h, 1 - xi).wait_send()
            r1_copy(s, h, xi).wait_send()
            r2_copy(s, h).wait_send()
    for s in visits:
        for h in halves:
            x_copy(s, h).wait_send()
            c_copy(s, h, 0).wait_send()
            c_copy(s, h, 1).wait_send()
            r3_copy(s, h).wait_send()
        for c in kv_copies(s):
            c.wait_send()

        @pl.when(forward_of(s)[0])
        def _():
            for h in halves:
                z_copy(s, h).wait_send()


def hand_on_kernel(a_ref, b_ref, c_ref, d_ref):
    c_ref[...] = a_ref[...]
    d_ref[...] = b_ref[...]


def fused(queries, keys, values, lambdas, head_gain, tokens, route_ids, route_weights, moe_gain, w_gate, w_up, w_down):
    n = lax.axis_size("ep")
    rows, width = tokens.shape
    cols = width // 4
    ff = w_gate.shape[2]
    vmem = pl.BlockSpec(memory_space=pltpu.VMEM)
    smem = pl.BlockSpec(memory_space=pltpu.SMEM)
    hbm = pl.BlockSpec(memory_space=pl.ANY)
    dma = pltpu.SemaphoreType.DMA
    results = pl.pallas_call(
        functools.partial(fused_kernel, n),
        out_shape=(
            jax.ShapeDtypeStruct((queries.shape[0], values.shape[1]), BF16),
            jax.ShapeDtypeStruct((rows, cols), BF16),
        ),
        in_specs=[vmem, vmem, vmem, smem, vmem, vmem, vmem, vmem, vmem, hbm, hbm, hbm],
        out_specs=(vmem, vmem),
        scratch_shapes=[
            pltpu.VMEM((width, ff), BF16),
            pltpu.VMEM((width, ff), BF16),
            pltpu.VMEM((ff, width), BF16),
            pltpu.VMEM((n, rows, width), BF16),
            pltpu.VMEM((n * keys.shape[0], keys.shape[1]), BF16),
            pltpu.VMEM((n * values.shape[0], values.shape[1]), BF16),
            pltpu.VMEM((rows, ff), BF16),
            pltpu.VMEM((n, rows, width), BF16),
            pltpu.VMEM((n, 2, rows, cols), BF16),
            pltpu.VMEM((n, rows, cols), F32),
            pltpu.VMEM((n, rows, cols), BF16),
            pltpu.VMEM((n, rows, cols), BF16),
            pltpu.VMEM((n, rows, cols), BF16),
            pltpu.VMEM((n, rows, cols), BF16),
            pltpu.VMEM((rows, -(-n // 8) * 8), F32),
            dma((3,)),
            dma((2, PIECES)),
            dma((n, PIECES)),
            dma((n, PIECES)),
            dma((n, PIECES)),
            dma((n, PIECES)),
            dma((2, n, PIECES)),
            dma((2, n, PIECES)),
            dma((2, n)),
            dma((2, n)),
            dma((2, n, PIECES)),
            dma((2, n, PIECES)),
            dma((n, PIECES)),
            dma((n, PIECES)),
            dma((n, PIECES)),
            dma((n, PIECES)),
        ],
        compiler_params=pltpu.CompilerParams(
            collective_id=0, has_side_effects=True, vmem_limit_bytes=60 * 1024 * 1024
        ),
        name="fused_layer",
    )(
        queries,
        keys,
        values,
        lambdas,
        head_gain,
        tokens,
        route_ids.T,
        route_weights.T,
        moe_gain,
        w_gate,
        w_up,
        w_down,
    )
    return pl.pallas_call(
        hand_on_kernel,
        out_shape=tuple(jax.ShapeDtypeStruct(r.shape, r.dtype) for r in results),
        in_specs=[vmem, vmem],
        out_specs=(vmem, vmem),
        name="hand_on",
    )(*results)


def on_device(
    queries,
    keys,
    values,
    lambdas,
    head_gain,
    tokens,
    route_ids,
    route_weights,
    moe_gain,
    w_gate,
    w_up,
    w_down,
):
    rows = tokens.shape[0]
    expert_count = w_gate.shape[0] * lax.axis_size("ep")
    slots = 2 * rows * route_ids.shape[1] // expert_count
    if w_gate.shape[0] == 1 and lax.axis_size("tp") == 4 and slots >= rows:
        return fused(
            queries, keys, values, lambdas, head_gain, tokens,
            route_ids, route_weights, moe_gain, w_gate, w_up, w_down,
        )
    heads_out = attend(queries, keys, values, lambdas, head_gain)
    expert_out = experts(tokens, route_ids, route_weights, moe_gain, w_gate, w_up, w_down)
    return (heads_out, expert_out)


def solution(mesh):
    in_specs = (
        P(("grp", "ep"), "tp"),
        P(("grp", "ep"), "tp"),
        P(("grp", "ep"), "tp"),
        P("tp"),
        P(),
        P(("grp", "ep"), None),
        P(("grp", "ep"), None),
        P(("grp", "ep"), None),
        P(),
        P("ep", None, "tp"),
        P("ep", None, "tp"),
        P("ep", "tp", None),
    )
    out_specs = (P(("grp", "ep"), "tp"), P(("grp", "ep"), "tp"))
    return jax.shard_map(
        on_device, mesh=mesh, in_specs=in_specs, out_specs=out_specs, check_vma=False
    )
```

profile of v0, /device:TPU:0, one launch (start us, length us, event | category | flops | bytes accessed | tf_op | source)
XLA Modules:
  0.0 55.4 jit_solution(15053745430539916427)
XLA Ops:
  0.6 53.1 %fused_layer.1 = (bf16[128,256]{1,0:T(8,128)(2,1)}, bf16[256,384]{1,0:T(8,128)(2,1)}) custom-call(bf16[128,256]{1,0:T(8,128)(2,1)} %q_ref.1, bf16[128,256]{1,0:T(8,128)(2,1)} %k_ref.1, bf16[128,256]{1,0:T(8,128)(2,1)} %v_ref.1, f32[2]{0:T(128)} %lam_ref.1, f32[128]{0:T(128)} %hgain_ref.1, bf16[256,1536]{1,0:T(8,128)(2,1)} %tok_ref.1, s32[2,256]{1,0:T(2,128)} %bitcast.2, ...), custom_call_target="tpu_custom_call" | custom-call | tf_op jit(solution)/shard_map/fused_layer/pallas_call | solution.py:524
  53.7 1.7 %hand_on.1 = (bf16[128,256]{1,0:T(8,128)(2,1)}, bf16[256,384]{1,0:T(8,128)(2,1)}) custom-call(bf16[128,256]{1,0:T(8,128)(2,1)} %get-tuple-element.4.a_ref, bf16[256,384]{1,0:T(8,128)(2,1)} %get-tuple-element.5.b_ref), custom_call_target="tpu_custom_call" | custom-call | tf_op jit(solution)/shard_map/hand_on/pallas_call | solution.py:583
where the time goes:
time: 55.5 us; the launch traced here: 55.4 us
  Pallas kernels  54.7 us (99%)
  between operations  0.64 us (1%)
    pallas_call x1, Pallas kernels, fused(): pl.pallas_call(functools.partial(fused_kernel, n), out_shape=(jax.ShapeDt...  53.1 us
    pallas_call x1, Pallas kernels, fused(): pl.pallas_call(hand_on_kernel, out_shape=tuple((jax.ShapeDtypeStruct(r.sh...  1.67 us

commit v1 on v0

v1 whole, which is shorter than its diff:
```python
import functools

import jax
import jax.numpy as jnp
from jax import lax
from jax.experimental import pallas as pl
from jax.experimental.pallas import tpu as pltpu
from jax.sharding import PartitionSpec as P

MESH = pl.DeviceIdType.MESH
F32 = jnp.float32
BF16 = jnp.bfloat16
PIECES = 4
OUTER_VISIT = 2

def attend(queries, keys, values, lambdas, head_gain):
    row_count = queries.shape[0]
    head_count = lambdas.shape[0]
    head_dim = queries.shape[1] // (2 * head_count)
    value_dim = values.shape[1] // head_count
    query_parts = queries.reshape(row_count, head_count, 2, head_dim)
    score_scale = head_dim ** (-0.5)
    running = jnp.full((head_count, 2, row_count), -1e30, jnp.float32)
    key_piece = lax.all_gather(keys, "ep", axis=0, tiled=True)
    value_piece = lax.all_gather(values, "ep", axis=0, tiled=True)
    count = key_piece.shape[0]
    key_parts = key_piece.reshape(count, head_count, 2, head_dim)
    value_parts = value_piece.reshape(count, head_count, value_dim)
    scores = (
        jnp.einsum("qhcd,khcd->hcqk", query_parts, key_parts, preferred_element_type=jnp.float32)
        * score_scale
    )
    newest = jnp.maximum(running, jnp.max(scores, axis=-1))
    weights_now = jnp.exp(scores - newest[..., None])
    totals = jnp.sum(weights_now, axis=-1)
    sums = jnp.einsum(
        "hcqk,khe->hcqe",
        weights_now.astype(jnp.bfloat16),
        value_parts,
        preferred_element_type=jnp.float32,
    )
    running, totals, sums = (newest, totals, sums)
    means = sums / totals[..., None]
    mixed = means[:, 0] - lambdas[:, None, None] * means[:, 1]
    scaled = mixed * lax.rsqrt(jnp.mean(mixed * mixed, axis=-1, keepdims=True) + 1e-06) * head_gain
    return (
        jnp.transpose(scaled, (1, 0, 2))
        .reshape(row_count, head_count * value_dim)
        .astype(jnp.bfloat16)
    )


def experts(tokens, route_ids, route_weights, moe_gain, w_gate, w_up, w_down):
    row_count, width = tokens.shape
    top_count = route_ids.shape[1]
    ep_size = lax.axis_size("ep")
    tp_size = lax.axis_size("tp")
    expert_count = w_gate.shape[0] * ep_size
    capacity = 2 * row_count * top_count // expert_count
    token_float = tokens.astype(jnp.float32)
    normed = (
        token_float
        * lax.rsqrt(jnp.mean(token_float * token_float, axis=1, keepdims=True) + 1e-06)
        * moe_gain
    ).astype(jnp.bfloat16)
    flat_ids = route_ids.reshape(-1)
    onehot = (flat_ids[:, None] == jnp.arange(expert_count, dtype=jnp.int32)[None, :]).astype(
        jnp.int32
    )
    earlier = jnp.cumsum(onehot, axis=0) - onehot
    position = jnp.sum(earlier * onehot, axis=1)
    slot_index = flat_ids * capacity + position
    owners = (
        jnp.full((expert_count * capacity,), row_count, jnp.int32)
        .at[slot_index]
        .set(jnp.arange(row_count * top_count, dtype=jnp.int32) // top_count)
    )
    padded = jnp.concatenate([normed, jnp.zeros((1, width), jnp.bfloat16)], axis=0)
    outgoing = padded[owners].reshape(expert_count, capacity, width)
    gate_mat = w_gate[0]
    up_mat = w_up[0]
    down_mat = w_down[0]
    slice_width = width // tp_size
    own_columns = lax.dynamic_slice_in_dim(
        outgoing, lax.axis_index("tp") * slice_width, slice_width, 2
    )
    arrived = lax.all_to_all(own_columns, "ep", split_axis=0, concat_axis=0, tiled=True)
    piece = lax.all_gather(arrived, "tp", axis=2, tiled=True)
    gate = jnp.einsum("scd,df->scf", piece, gate_mat, preferred_element_type=jnp.float32)
    upward = jnp.einsum("scd,df->scf", piece, up_mat, preferred_element_type=jnp.float32)
    hidden = (jax.nn.silu(gate) * upward).astype(jnp.bfloat16)
    flat_hidden = hidden.reshape(-1, hidden.shape[2])
    summed = lax.psum_scatter(
        jnp.einsum("fd,sf->ds", down_mat, flat_hidden, preferred_element_type=jnp.float32).astype(
            jnp.bfloat16
        ),
        "tp",
        scatter_dimension=0,
        tiled=True,
    )
    back = lax.all_to_all(summed, "ep", split_axis=1, concat_axis=1, tiled=True)
    picked = (
        jnp.take(back, slot_index, axis=1).astype(jnp.float32).reshape(-1, row_count, top_count)
    )
    combined = jnp.einsum("drk,rk->rd", picked, route_weights)
    return combined.astype(jnp.bfloat16)


def visit_order(n):
    def key(e):
        left = 2 * e < n
        outward = (lambda s: s < e) if left else (lambda s: s > e)
        return lambda s: (outward(s), abs(s - e))

    return [sorted((s for s in range(n) if s != e), key=key(e)) for e in range(n)]


def fused_kernel(
    n,
    q_hbm,
    k_hbm,
    v_hbm,
    lam_hbm,
    hgain_hbm,
    tok_hbm,
    ids_hbm,
    rw_hbm,
    mgain_hbm,
    wg_hbm,
    wu_hbm,
    wd_hbm,
    heads_ref,
    out_ref,
    wg,
    wu,
    wd,
    q_ref,
    lam_ref,
    hgain_ref,
    tok_ref,
    ids_ref,
    rw_ref,
    mgain_ref,
    gathered,
    kv,
    hid,
    part,
    core_in,
    s_own,
    s_out,
    x_in,
    t_out,
    ret,
    z_out,
    z_in,
    out_weights,
    wsem,
    tok_sem,
    in_sem,
    own_send,
    z_send,
    z_recv,
    x_send,
    x_recv,
    c_send,
    c_recv,
    kv_own_send,
    kv_send,
    kv_recv,
    r1_send,
    r1_recv,
    r2_send,
    r2_recv,
    r3_send,
    r3_recv,
    zo_send,
    zo_recv,
):
    e = lax.axis_index("ep")
    t = lax.axis_index("tp")
    xi = t // 2
    ci = lax.rem(t, 2)
    core_peer = {"tp": 2 * xi + 1 - ci}
    tx = 2 * (1 - xi) + ci
    x_peer = {"tp": tx}
    rows, width = tok_ref.shape
    cols = width // 4
    kv_rows = k_hbm.shape[0]
    has_left = e > 0
    has_right = e < n - 1
    inner = jnp.logical_and(has_left, has_right)
    outer = jnp.logical_not(inner)
    left_half = 2 * e < n
    inward = {"ep": jnp.clip(jnp.where(left_half, e + 1, e - 1), 0, n - 1)}
    outward = {"ep": jnp.clip(jnp.where(left_half, e - 1, e + 1), 0, n - 1)}

    def colblock(j):
        return pl.ds(pl.multiple_of(j * cols, 128), cols)

    def remote(src, dst, ss, rs, dev):
        return pltpu.make_async_remote_copy(
            src_ref=src, dst_ref=dst, send_sem=ss, recv_sem=rs, device_id=dev, device_id_type=MESH
        )

    barrier = pltpu.get_barrier_semaphore()
    pl.semaphore_signal(barrier, inc=1, device_id=inward, device_id_type=MESH)

    @pl.when(inner)
    def _():
        pl.semaphore_signal(barrier, inc=1, device_id=outward, device_id_type=MESH)

    pl.semaphore_signal(barrier, inc=1, device_id=core_peer, device_id_type=MESH)
    pl.semaphore_signal(barrier, inc=1, device_id=x_peer, device_id_type=MESH)
    greeted = 3 + inner.astype(jnp.int32)

    halves = range(PIECES)
    early, late = halves[: PIECES // 2], halves[PIECES // 2 :]
    hr = rows // PIECES

    def half(h):
        return pl.ds(h * hr, hr)

    own_kv = pl.ds(pl.multiple_of(e * kv_rows, kv_rows), kv_rows)
    k_width = k_hbm.shape[1]
    v_width = v_hbm.shape[1]
    gain_in = pltpu.make_async_copy(mgain_hbm, mgain_ref, in_sem.at[0])
    gain_in.start()
    tokens_in = pltpu.make_async_copy(tok_hbm, tok_ref, tok_sem.at[0])
    tokens_in.start()
    weights = [
        pltpu.make_async_copy(a, b, wsem.at[i])
        for i, (a, b) in enumerate(((wg_hbm.at[0], wg), (wu_hbm.at[0], wu), (wd_hbm.at[0], wd)))
    ]
    kv_in = [
        pltpu.make_async_copy(k_hbm, kv.at[own_kv, pl.ds(0, k_width)], in_sem.at[1]),
        pltpu.make_async_copy(v_hbm, kv.at[own_kv, pl.ds(k_width, v_width)], in_sem.at[2]),
    ]
    others_in = [
        pltpu.make_async_copy(a, b, in_sem.at[i + 3])
        for i, (a, b) in enumerate(
            ((ids_hbm, ids_ref), (rw_hbm, rw_ref), (q_hbm, q_ref), (lam_hbm, lam_ref), (hgain_hbm, hgain_ref))
        )
    ]

    def normalize(h):
        step = 32

        @pl.loop(0, hr // step)
        def _(i):
            sl = pl.ds(pl.multiple_of(h * hr + i * step, step), step)
            v = tok_ref[sl, :].astype(F32)
            scale = lax.rsqrt(jnp.mean(v * v, axis=1, keepdims=True) + 1e-06)
            gathered[e, sl, :] = (v * scale * mgain_ref[...]).astype(BF16)

    def own_tok(side, h):
        blk = gathered.at[e, half(h), colblock(t)]
        return remote(blk, blk, own_send.at[0], z_recv.at[e, h], (inward, outward)[side])

    def own_tok2(h):
        blk = gathered.at[e, half(h), colblock(tx)]
        return remote(blk, blk, own_send.at[0], x_recv.at[e, h], inward)

    def own_kv_copy(side):
        blk = kv.at[own_kv]
        return remote(blk, blk, kv_own_send.at[0], kv_recv.at[e], (inward, outward)[side])

    orders = visit_order(n)

    def nth(k):
        s = jnp.int32(orders[0][k])
        for i in range(1, n):
            s = jnp.where(e == i, jnp.int32(orders[i][k]), s)
        return s

    visits = [nth(k) for k in range(n - 1)]

    def onward(k):
        return inward if k == OUTER_VISIT else outward

    def z_copy(k, h):
        blk = gathered.at[visits[k], half(h), colblock(t)]
        return remote(blk, blk, z_send.at[0], z_recv.at[visits[k], h], onward(k))

    def kv_copy(k):
        s = visits[k]
        blk = kv.at[pl.ds(pl.multiple_of(s * kv_rows, kv_rows), kv_rows)]
        return remote(blk, blk, kv_send.at[0], kv_recv.at[s], onward(k))

    def x_copy(s, h):
        blk = gathered.at[s, half(h), colblock(t)]
        return remote(blk, blk, x_send.at[0], x_recv.at[s, h], x_peer)

    def c_copy(s, h, which):
        blk = gathered.at[s, half(h), colblock((t, tx)[which])]
        return remote(blk, blk, c_send.at[0], c_recv.at[s], core_peer)

    def r1_copy(s, xx):
        return remote(
            part.at[s, :, colblock(2 * xx + 1 - ci)],
            core_in.at[s, xx],
            r1_send.at[0],
            r1_recv.at[xx, s],
            core_peer,
        )

    def r2_copy(s, h):
        return remote(
            s_out.at[s, half(h)], x_in.at[s, half(h)], r2_send.at[s], r2_recv.at[s, h], x_peer
        )

    def r3_copy(s, h):
        return remote(
            t_out.at[s, half(h)],
            ret.at[e, half(h)],
            r3_send.at[0],
            r3_recv.at[e, h],
            {"ep": s},
        )

    def r3_back(s, h):
        return remote(
            t_out.at[s, half(h)],
            ret.at[s, half(h)],
            r3_send.at[0],
            r3_recv.at[s, h],
            {"ep": s},
        )

    def zo_copy(i, h):
        return remote(
            z_out.at[i, half(h)], z_in.at[i, half(h)], zo_send.at[0], zo_recv.at[i, h], inward
        )

    ff = wg.shape[1]
    nb = ff // 3

    def up_step(s, b):
        sl = pl.ds(b * nb, nb)
        g = jnp.dot(gathered[s], wg[:, sl], preferred_element_type=F32)
        u = jnp.dot(gathered[s], wu[:, sl], preferred_element_type=F32)
        hid[:, sl] = (g / (1.0 + jnp.exp(-g)) * u).astype(BF16)

    def down_step(s, j):
        sl = colblock(j)
        part[s, :, sl] = jnp.dot(hid[...], wd[:, sl], preferred_element_type=F32).astype(BF16)

    def down_far(s):
        down_step(s, 2 * (1 - xi) + 1 - ci)
        r1_copy(s, 1 - xi).start()
        down_step(s, tx)

    def down_near(s):
        down_step(s, 2 * xi + 1 - ci)
        r1_copy(s, xi).start()
        down_step(s, t)

    def across(s, h):
        return part[s, half(h), colblock(tx)].astype(F32) + core_in[s, 1 - xi, half(h)].astype(F32)

    def along(s, h):
        return part[s, half(h), colblock(t)].astype(F32) + core_in[s, xi, half(h)].astype(F32)

    def reduce_core(s):
        r1_copy(s, 1 - xi).wait_recv()
        for h in halves:
            s_out[s, half(h)] = across(s, h).astype(BF16)
            r2_copy(s, h).start()

    def reduce_z(s):
        r1_copy(s, 1 - xi).wait_recv()
        for h in halves:
            z_out[0, half(h)] = across(s, h).astype(BF16)
            zo_copy(0, h).start()
        r1_copy(s, xi).wait_recv()
        for h in halves:
            z_out[1, half(h)] = along(s, h).astype(BF16)
            zo_copy(1, h).start()

    def own_sums():
        r1_copy(e, 1 - xi).wait_recv()
        r1_copy(e, xi).wait_recv()

    def reduce_own(h, joined):
        w = out_weights[half(h), 0:1]
        there = across(e, h) * w
        here = along(e, h) * w
        if joined:
            zo_copy(0, h).wait_recv()
            zo_copy(1, h).wait_recv()
            v = out_weights[half(h), OUTER_VISIT + 1 : OUTER_VISIT + 2]
            there = there + z_in[0, half(h)].astype(F32) * v
            here = here + z_in[1, half(h)].astype(F32) * v
        s_out[e, half(h)] = there.astype(BF16)
        r2_copy(e, h).start()
        s_own[half(h)] = here

    def reduce_x(s, h):
        if h == 0:
            r1_copy(s, xi).wait_recv()
        r2_copy(s, h).wait_recv()
        t_out[s, half(h)] = (along(s, h) + x_in[s, half(h)].astype(F32)).astype(BF16)
        r3_copy(s, h).start()

    def arrive(k, h, x=True):
        z_copy(k, h).wait_recv()
        if x:
            x_copy(visits[k], h).start()
        c_copy(visits[k], h, 0).start()

    def relay(k, h, x=True):
        z_copy(k, h).wait_recv()
        z_copy(k, h).start()
        if x:
            x_copy(visits[k], h).start()
        c_copy(visits[k], h, 0).start()

    def cross(k, h):
        x_copy(visits[k], h).wait_recv()
        c_copy(visits[k], h, 1).start()

    def waiter(ref, ss, rs):
        return remote(ref, ref, ss, rs, core_peer)

    def ready(s):
        waiter(gathered.at[s, :, pl.ds(0, 2 * cols)], c_send.at[0], c_recv.at[s]).wait_recv()

    def attend(h):
        heads = lam_ref.shape[0]
        vd = v_width // heads
        hd = q_ref.shape[1] // (2 * heads)
        qr = q_ref.shape[0]
        first = lax.broadcasted_iota(jnp.int32, (qr, 2 * hd), 1) < hd
        q = q_ref[:, h * 2 * hd : (h + 1) * 2 * hd].astype(F32)
        both = jnp.concatenate(
            [jnp.where(first, q, 0.0).astype(BF16), jnp.where(first, 0.0, q).astype(BF16)], axis=0
        )
        kh = kv[:, h * 2 * hd : (h + 1) * 2 * hd]
        vh = kv[:, k_width + h * vd : k_width + (h + 1) * vd]
        scores = lax.dot_general(
            both, kh, (((1,), (1,)), ((), ())), preferred_element_type=F32
        ) * (hd ** (-0.5))
        ex = jnp.exp(scores - jnp.max(scores, axis=1, keepdims=True))
        tot = jnp.sum(ex, axis=1, keepdims=True)
        sums = jnp.dot(ex.astype(BF16), vh, preferred_element_type=F32) / tot
        mixed = sums[:qr] - lam_ref[h] * sums[qr:]
        norm = lax.rsqrt(jnp.mean(mixed * mixed, axis=1, keepdims=True) + 1e-06)
        heads_ref[:, h * vd : (h + 1) * vd] = (mixed * norm * hgain_ref[...]).astype(BF16)

    def add_back(k, h, end):
        r3_back(visits[k], h).wait_recv()
        w = out_weights[half(h), k + 1 : k + 2]
        total = s_own[half(h)] + ret[visits[k], half(h)].astype(F32) * w
        if end:
            out_ref[half(h), :] = total.astype(BF16)
        else:
            s_own[half(h)] = total

    def on_inner(fn):
        pl.when(inner)(fn)

    def on_outer(fn):
        pl.when(outer)(fn)

    def at(out, inn):
        if out:

            @on_outer
            def _():
                for f, *args in out:
                    f(*args)

        if inn:

            @on_inner
            def _():
                for f, *args in inn:
                    f(*args)

    def start_kv(side):
        own_kv_copy(side).start()

    def take_kv(k):
        kv_copy(k).wait_recv()

    def pass_kv(k):
        kv_copy(k).wait_recv()
        kv_copy(k).start()

    def start_tok2(h):
        own_tok2(h).start()

    def relays(h):
        relay(2, h, False)
        relay(0, h)

    gain_in.wait()
    for c in kv_in + others_in:
        c.start()
    tokens_in.wait()
    for c in weights:
        c.start()
    for h in halves:
        normalize(h)
        if h == 0:
            pl.semaphore_wait(barrier, greeted)
        own_tok(0, h).start()

        @on_inner
        def _():
            own_tok(1, h).start()

    for c in kv_in + others_in:
        c.wait()
    ids = ids_ref[...]
    rw = rw_ref[...]
    lines = [jnp.sum(jnp.where(ids == x, rw, 0.0), axis=0, keepdims=True) for x in [e] + visits]
    pad = (-len(lines)) % 8
    lines.append(jnp.zeros((pad, rows), F32))
    out_weights[...] = jnp.concatenate(lines, axis=0).T

    for c in weights:
        c.wait()
    v0, v1, v2 = visits
    up_step(e, 0)
    at([(arrive, 0, 0), (start_tok2, 0)], [(relays, 0)])
    up_step(e, 1)
    at([(arrive, 0, 1), (start_tok2, 1)], [(relays, 1)])
    up_step(e, 2)
    at([(arrive, 0, 2), (start_tok2, 2)], [(relays, 2)])
    down_far(e)
    at(
        [(start_tok2, 3), (arrive, 0, 3), (start_kv, 0), (cross, 0, 0)],
        [(relays, 3), (cross, 0, 0)],
    )
    down_near(e)
    at(
        [
            (arrive, 1, 0), (cross, 0, 1), (arrive, 1, 1), (cross, 0, 2), (arrive, 1, 2),
            (cross, 0, 3),
        ],
        [
            (relay, 1, 0), (cross, 0, 1), (cross, 2, 0), (relay, 1, 1), (cross, 0, 2), (cross, 2, 1),
            (relay, 1, 2), (cross, 0, 3), (cross, 2, 2), (start_kv, 0),
        ],
    )
    ready(v0)
    up_step(v0, 0)
    at([(arrive, 1, 3), (cross, 1, 0)], [(relay, 1, 3), (cross, 2, 3), (start_kv, 1), (cross, 1, 0)])
    up_step(v0, 1)
    at([(arrive, 2, 0), (cross, 1, 1)], [(cross, 1, 1)])
    up_step(v0, 2)
    at([(arrive, 2, 1), (cross, 1, 2)], [(cross, 1, 2)])
    down_far(v0)
    at([(arrive, 2, 2), (cross, 1, 3)], [(cross, 1, 3)])
    down_near(v0)
    own_sums()
    at([(arrive, 2, 3)] + [(reduce_own, h, False) for h in early], [(reduce_core, v0)])
    ready(v1)
    up_step(v1, 0)
    at([(reduce_z, v0), (cross, 2, 0), (cross, 2, 1)], [(pass_kv, 2)])
    up_step(v1, 1)
    at([(cross, 2, 2)], [])
    up_step(v1, 2)
    down_far(v1)
    at([(cross, 2, 3)], [(pass_kv, 0)])
    down_near(v1)
    reduce_core(v1)
    at([], [(reduce_x, v0, h) for h in early])
    ready(v2)
    up_step(v2, 0)
    at([], [(reduce_x, v0, 2)])
    up_step(v2, 1)
    at([], [(pass_kv, 1)])
    up_step(v2, 2)
    at([], [(reduce_x, v0, 3)])
    down_far(v2)
    at([(reduce_x, v1, 0)], [])
    down_near(v2)
    reduce_core(v2)
    reduce_rest = [(reduce_x, v1, h) for h in early]
    at(reduce_rest[1:], reduce_rest)
    at([(take_kv, k) for k in range(n - 1)], [])
    attend(0)
    reduce_x(v1, 2)
    for h in range(1, lam_ref.shape[0]):
        attend(h)
    reduce_x(v1, 3)

    def settle(joined, hs):
        waiter(s_out.at[v2], r2_send.at[v2], r2_recv.at[v2, 0]).wait_send()
        for h in hs:
            reduce_own(h, joined)
        for h in halves:
            reduce_x(v2, h)

    at([(settle, False, late)], [(settle, True, halves)])

    for h in halves:
        r2_copy(e, h).wait_recv()
        s_own[half(h)] = s_own[half(h)] + x_in[e, half(h)].astype(F32)

    def gather_back(ks):
        for k in ks:
            for h in halves:
                add_back(k, h, k == ks[-1])

    @on_outer
    def _():
        gather_back((1, 0, 2))

    @on_inner
    def _():
        gather_back((0, 1))

    def sent(ref, sem):
        waiter(ref, sem, c_recv.at[e]).wait_send()

    quarter, double = pl.ds(0, cols), pl.ds(0, 2 * cols)
    sent(part.at[:, :, double], r1_send.at[0])
    sent(gathered.at[pl.ds(0, 3), :, double], c_send.at[0])
    sent(gathered.at[pl.ds(0, 2), :, quarter], own_send.at[0])
    sent(s_out.at[e], r2_send.at[e])
    sent(s_out.at[v1], r2_send.at[v1])

    @on_outer
    def _():
        sent(kv.at[pl.ds(0, kv_rows)], kv_own_send.at[0])
        sent(gathered.at[pl.ds(0, 3), :, quarter], x_send.at[0])
        sent(z_out, zo_send.at[0])
        sent(t_out.at[pl.ds(0, 2)], r3_send.at[0])

    @on_inner
    def _():
        sent(kv.at[pl.ds(0, 2 * kv_rows)], kv_own_send.at[0])
        sent(kv.at[pl.ds(0, 3 * kv_rows)], kv_send.at[0])
        sent(gathered.at[pl.ds(0, 3), :, quarter], z_send.at[0])
        sent(gathered.at[pl.ds(0, 2), :, quarter], x_send.at[0])
        sent(s_out.at[v0], r2_send.at[v0])
        sent(t_out.at[pl.ds(0, 3)], r3_send.at[0])


def hand_on_kernel(a_ref, b_ref, c_ref, d_ref):
    c_ref[...] = a_ref[...]
    d_ref[...] = b_ref[...]


def fused(queries, keys, values, lambdas, head_gain, tokens, route_ids, route_weights, moe_gain, w_gate, w_up, w_down):
    n = lax.axis_size("ep")
    rows, width = tokens.shape
    cols = width // 4
    ff = w_gate.shape[2]
    vmem = pl.BlockSpec(memory_space=pltpu.VMEM)
    hbm = pl.BlockSpec(memory_space=pltpu.HBM)
    dma = pltpu.SemaphoreType.DMA
    results = pl.pallas_call(
        functools.partial(fused_kernel, n),
        out_shape=(
            pltpu.VMEM((queries.shape[0], values.shape[1]), BF16),
            pltpu.VMEM((rows, cols), BF16),
        ),
        in_specs=[hbm] * 12,
        out_specs=(vmem, vmem),
        scratch_shapes=[
            pltpu.VMEM((width, ff), BF16),
            pltpu.VMEM((width, ff), BF16),
            pltpu.VMEM((ff, width), BF16),
            pltpu.VMEM(queries.shape, BF16),
            pltpu.SMEM(lambdas.shape, F32),
            pltpu.VMEM(head_gain.shape, F32),
            pltpu.VMEM((rows, width), BF16),
            pltpu.VMEM(route_ids.shape[::-1], jnp.int32),
            pltpu.VMEM(route_weights.shape[::-1], F32),
            pltpu.VMEM(moe_gain.shape, F32),
            pltpu.VMEM((n, rows, width), BF16),
            pltpu.VMEM((n * keys.shape[0], keys.shape[1] + values.shape[1]), BF16),
            pltpu.VMEM((rows, ff), BF16),
            pltpu.VMEM((n, rows, width), BF16),
            pltpu.VMEM((n, 2, rows, cols), BF16),
            pltpu.VMEM((rows, cols), F32),
            pltpu.VMEM((n, rows, cols), BF16),
            pltpu.VMEM((n, rows, cols), BF16),
            pltpu.VMEM((n, rows, cols), BF16),
            pltpu.VMEM((n, rows, cols), BF16),
            pltpu.VMEM((2, rows, cols), BF16),
            pltpu.VMEM((2, rows, cols), BF16),
            pltpu.VMEM((rows, -(-n // 8) * 8), F32),
            dma((3,)),
            dma((1,)),
            dma((8,)),
            dma((1,)),
            dma((1,)),
            dma((n, PIECES)),
            dma((1,)),
            dma((n, PIECES)),
            dma((1,)),
            dma((n,)),
            dma((1,)),
            dma((1,)),
            dma((n,)),
            dma((1,)),
            dma((2, n)),
            dma((n,)),
            dma((n, PIECES)),
            dma((1,)),
            dma((n, PIECES)),
            dma((1,)),
            dma((2, PIECES)),
        ],
        compiler_params=pltpu.CompilerParams(
            collective_id=0, has_side_effects=True, vmem_limit_bytes=60 * 1024 * 1024
        ),
        name="fused_layer",
    )(
        queries,
        keys,
        values,
        lambdas,
        head_gain,
        tokens,
        route_ids.T,
        route_weights.T,
        moe_gain,
        w_gate,
        w_up,
        w_down,
    )
    return pl.pallas_call(
        hand_on_kernel,
        out_shape=tuple(jax.ShapeDtypeStruct(r.shape, r.dtype) for r in results),
        in_specs=[vmem, vmem],
        out_specs=(vmem, vmem),
        compiler_params=pltpu.CompilerParams(vmem_limit_bytes=4 * 1024 * 1024),
        name="hand_on",
    )(*results)


def on_device(
    queries,
    keys,
    values,
    lambdas,
    head_gain,
    tokens,
    route_ids,
    route_weights,
    moe_gain,
    w_gate,
    w_up,
    w_down,
):
    rows = tokens.shape[0]
    expert_count = w_gate.shape[0] * lax.axis_size("ep")
    slots = 2 * rows * route_ids.shape[1] // expert_count
    if w_gate.shape[0] == 1 and lax.axis_size("tp") == lax.axis_size("ep") == 4 and slots >= rows:
        return fused(
            queries, keys, values, lambdas, head_gain, tokens,
            route_ids, route_weights, moe_gain, w_gate, w_up, w_down,
        )
    heads_out = attend(queries, keys, values, lambdas, head_gain)
    expert_out = experts(tokens, route_ids, route_weights, moe_gain, w_gate, w_up, w_down)
    return (heads_out, expert_out)


def solution(mesh):
    in_specs = (
        P(("grp", "ep"), "tp"),
        P(("grp", "ep"), "tp"),
        P(("grp", "ep"), "tp"),
        P("tp"),
        P(),
        P(("grp", "ep"), None),
        P(("grp", "ep"), None),
        P(("grp", "ep"), None),
        P(),
        P("ep", None, "tp"),
        P("ep", None, "tp"),
        P("ep", "tp", None),
    )
    out_specs = (P(("grp", "ep"), "tp"), P(("grp", "ep"), "tp"))
    return jax.shard_map(
        on_device, mesh=mesh, in_specs=in_specs, out_specs=out_specs, check_vma=False
    )
```

time: 55.5 us -> 49.3 us (0.89)
  Pallas kernels: 54.7 us -> 48.5 us
    pallas_call x1, Pallas kernels: 53.1 us -> 47.8 us  [fused(): pl.pallas_call(functools.partial(fused_kernel, n), out_shape=(pltpu.VMEM(...]
    pallas_call x1, Pallas kernels: 1.67 us -> 0.72 us  [fused(): pl.pallas_call(hand_on_kernel, out_shape=tuple((jax.ShapeDtypeStruct(r.sh...]
where the time goes in v1:
time: 49.3 us; the launch traced here: 49.1 us
  Pallas kernels  48.5 us (98%)
  between operations  0.64 us (1%)
    pallas_call x1, Pallas kernels, fused(): pl.pallas_call(functools.partial(fused_kernel, n), out_shape=(pltpu.VMEM(...  47.8 us

profile of v1, /device:TPU:0, one launch (start us, length us, event | category | flops | bytes accessed | tf_op | source)
XLA Modules:
  0.0 49.1 jit_solution(4277872105167406569)
XLA Ops:
  0.6 47.8 %fused_layer.1 = (bf16[128,256]{1,0:T(8,128)(2,1)S(1)}, bf16[256,384]{1,0:T(8,128)(2,1)S(1)}) custom-call(bf16[128,256]{1,0:T(8,128)(2,1)} %q_hbm.1, bf16[128,256]{1,0:T(8,128)(2,1)} %k_hbm.1, bf16[128,256]{1,0:T(8,128)(2,1)} %v_hbm.1, f32[2]{0:T(128)} %lam_hbm.1, f32[128]{0:T(128)} %hgain_hbm.1, bf16[256,1536]{1,0:T(8,128)(2,1)} %tok_hbm.1, ...), custom_call_target="tpu_custom_call" | custom-call | tf_op jit(solution)/shard_map/fused_layer/pallas_call | solution.py:655
  48.4 0.7 %hand_on.1 = (bf16[128,256]{1,0:T(8,128)(2,1)}, bf16[256,384]{1,0:T(8,128)(2,1)}) custom-call(bf16[128,256]{1,0:T(8,128)(2,1)S(1)} %get-tuple-element.4.a_ref, bf16[256,384]{1,0:T(8,128)(2,1)S(1)} %get-tuple-element.5.b_ref), custom_call_target="tpu_custom_call" | custom-call | tf_op jit(solution)/shard_map/hand_on/pallas_call | solution.py:727

commit v2 on v1

--- a/solution.py
+++ b/solution.py
@@ -11,7 +11,7 @@
 F32 = jnp.float32
 BF16 = jnp.bfloat16
 PIECES = 4
-OUTER_VISIT = 2
+OUTER_VISIT = 0
 
 def attend(queries, keys, values, lambdas, head_gain):
     row_count = queries.shape[0]
@@ -109,8 +109,9 @@
 def visit_order(n):
     def key(e):
         left = 2 * e < n
-        outward = (lambda s: s < e) if left else (lambda s: s > e)
-        return lambda s: (outward(s), abs(s - e))
+        if e in (0, n - 1):
+            return lambda s: (False, abs(s - e))
+        return lambda s: (s > e if left else s < e, -abs(s - e))
 
     return [sorted((s for s in range(n) if s != e), key=key(e)) for e in range(n)]
 
@@ -153,7 +154,11 @@
     ret,
     z_out,
     z_in,
-    out_weights,
+    join,
+    lines,
+    tables,
+    own_weights,
+    weights_at,
     wsem,
     tok_sem,
     in_sem,
@@ -175,6 +180,10 @@
     r3_recv,
     zo_send,
     zo_recv,
+    join_send,
+    join_recv,
+    tab_send,
+    tab_recv,
 ):
     e = lax.axis_index("ep")
     t = lax.axis_index("tp")
@@ -225,8 +234,12 @@
     v_width = v_hbm.shape[1]
     gain_in = pltpu.make_async_copy(mgain_hbm, mgain_ref, in_sem.at[0])
     gain_in.start()
-    tokens_in = pltpu.make_async_copy(tok_hbm, tok_ref, tok_sem.at[0])
-    tokens_in.start()
+    tokens_in = [
+        pltpu.make_async_copy(tok_hbm.at[half(h)], tok_ref.at[half(h)], tok_sem.at[h])
+        for h in halves
+    ]
+    for c in tokens_in:
+        c.start()
     weights = [
         pltpu.make_async_copy(a, b, wsem.at[i])
         for i, (a, b) in enumerate(((wg_hbm.at[0], wg), (wu_hbm.at[0], wu), (wd_hbm.at[0], wd)))
@@ -308,27 +321,25 @@
             s_out.at[s, half(h)], x_in.at[s, half(h)], r2_send.at[s], r2_recv.at[s, h], x_peer
         )
 
-    def r3_copy(s, h):
+    def ret_copy(s, h):
         return remote(
-            t_out.at[s, half(h)],
-            ret.at[e, half(h)],
-            r3_send.at[0],
-            r3_recv.at[e, h],
-            {"ep": s},
+            t_out.at[s, half(h)], ret.at[e, half(h)], r3_send.at[0], r3_recv.at[e], {"ep": s}
         )
 
-    def r3_back(s, h):
+    def join_copy(s, h):
         return remote(
-            t_out.at[s, half(h)],
-            ret.at[s, half(h)],
-            r3_send.at[0],
-            r3_recv.at[s, h],
-            {"ep": s},
+            t_out.at[s, half(h)], join.at[half(h)], join_send.at[0], join_recv.at[h], inward
         )
+
+    def tab_copy(s):
+        return remote(lines, tables.at[e], tab_send.at[0], tab_recv.at[e], {"ep": s})
+
+    def tab_back(s):
+        return remote(lines, tables.at[s], tab_send.at[0], tab_recv.at[s], {"ep": s})
 
     def zo_copy(i, h):
         return remote(
-            z_out.at[i, half(h)], z_in.at[i, half(h)], zo_send.at[0], zo_recv.at[i, h], inward
+            z_out.at[i, half(h)], z_in.at[i, half(h)], zo_send.at[0], zo_recv.at[0], inward
         )
 
     ff = wg.shape[1]
@@ -366,40 +377,65 @@
             s_out[s, half(h)] = across(s, h).astype(BF16)
             r2_copy(s, h).start()
 
-    def reduce_z(s):
+    def reduce_z_far(s):
         r1_copy(s, 1 - xi).wait_recv()
         for h in halves:
             z_out[0, half(h)] = across(s, h).astype(BF16)
             zo_copy(0, h).start()
+
+    def reduce_z_near(s):
         r1_copy(s, xi).wait_recv()
         for h in halves:
             z_out[1, half(h)] = along(s, h).astype(BF16)
             zo_copy(1, h).start()
 
+    def take_zo():
+        waiter(z_in, zo_send.at[0], zo_recv.at[0]).wait_recv()
+
     def own_sums():
         r1_copy(e, 1 - xi).wait_recv()
         r1_copy(e, xi).wait_recv()
 
     def reduce_own(h, joined):
-        w = out_weights[half(h), 0:1]
+        w = own_weights[half(h), 0:1]
         there = across(e, h) * w
         here = along(e, h) * w
         if joined:
-            zo_copy(0, h).wait_recv()
-            zo_copy(1, h).wait_recv()
-            v = out_weights[half(h), OUTER_VISIT + 1 : OUTER_VISIT + 2]
+            v = own_weights[half(h), 1:2]
             there = there + z_in[0, half(h)].astype(F32) * v
             here = here + z_in[1, half(h)].astype(F32) * v
         s_out[e, half(h)] = there.astype(BF16)
         r2_copy(e, h).start()
         s_own[half(h)] = here
 
-    def reduce_x(s, h):
+    def finish(k, h, hand, joined=False):
+        s = visits[k]
         if h == 0:
             r1_copy(s, xi).wait_recv()
         r2_copy(s, h).wait_recv()
-        t_out[s, half(h)] = (along(s, h) + x_in[s, half(h)].astype(F32)).astype(BF16)
-        r3_copy(s, h).start()
+        total = (along(s, h) + x_in[s, half(h)].astype(F32)) * weights_at[half(h), k : k + 1]
+        if joined:
+            join_copy(s, h).wait_recv()
+            total = total + join[half(h)].astype(F32)
+        t_out[s, half(h)] = total.astype(BF16)
+        hand(s, h).start()
+
+    def columns(picked):
+        pad = jnp.zeros(((-len(picked)) % 8, rows), F32)
+        return jnp.concatenate(picked + [pad], axis=0).T
+
+    def line_of(table, x):
+        is_x = lax.broadcasted_iota(jnp.int32, table.shape, 0) == x
+        return jnp.sum(jnp.where(is_x, table, 0.0), axis=0, keepdims=True)
+
+    def weigh():
+        for s in visits:
+            tab_back(s).wait_recv()
+        weights_at[...] = columns([line_of(tables[s], e) for s in visits])
+
+    def start_tables():
+        for s in visits:
+            tab_copy(s).start()
 
     def arrive(k, h, x=True):
         z_copy(k, h).wait_recv()
@@ -447,14 +483,15 @@
         heads_ref[:, h * vd : (h + 1) * vd] = (mixed * norm * hgain_ref[...]).astype(BF16)
 
     def add_back(k, h, end):
-        r3_back(visits[k], h).wait_recv()
-        w = out_weights[half(h), k + 1 : k + 2]
-        total = s_own[half(h)] + ret[visits[k], half(h)].astype(F32) * w
+        total = s_own[half(h)] + ret[visits[k], half(h)].astype(F32)
         if end:
             out_ref[half(h), :] = total.astype(BF16)
         else:
             s_own[half(h)] = total
 
+    def drained(k):
+        waiter(s_out.at[visits[k]], r2_send.at[visits[k]], r2_recv.at[visits[k], 0]).wait_send()
+
     def on_inner(fn):
         pl.when(inner)(fn)
 
@@ -490,18 +527,21 @@
         own_tok2(h).start()
 
     def relays(h):
-        relay(2, h, False)
-        relay(0, h)
+        relay(OUTER_VISIT, h, False)
+        relay(2, h)
 
     gain_in.wait()
     for c in kv_in + others_in:
         c.start()
-    tokens_in.wait()
-    for c in weights:
-        c.start()
     for h in halves:
+        if h == 0:
+            tokens_in[h].wait()
         normalize(h)
         if h == 0:
+            for c in tokens_in[1:]:
+                c.wait()
+            for c in weights:
+                c.start()
             pl.semaphore_wait(barrier, greeted)
         own_tok(0, h).start()
 
@@ -513,10 +553,9 @@
         c.wait()
     ids = ids_ref[...]
     rw = rw_ref[...]
-    lines = [jnp.sum(jnp.where(ids == x, rw, 0.0), axis=0, keepdims=True) for x in [e] + visits]
-    pad = (-len(lines)) % 8
-    lines.append(jnp.zeros((pad, rows), F32))
-    out_weights[...] = jnp.concatenate(lines, axis=0).T
+    each = [jnp.sum(jnp.where(ids == x, rw, 0.0), axis=0, keepdims=True) for x in range(n)]
+    lines[...] = jnp.concatenate(each + [jnp.zeros((lines.shape[0] - n, rows), F32)], axis=0)
+    own_weights[...] = columns([line_of(lines[...], e), line_of(lines[...], visits[OUTER_VISIT])])
 
     for c in weights:
         c.wait()
@@ -539,61 +578,63 @@
             (cross, 0, 3),
         ],
         [
-            (relay, 1, 0), (cross, 0, 1), (cross, 2, 0), (relay, 1, 1), (cross, 0, 2), (cross, 2, 1),
-            (relay, 1, 2), (cross, 0, 3), (cross, 2, 2), (start_kv, 0),
+            (relay, 1, 0), (start_tables,), (cross, 0, 1), (cross, 2, 0), (relay, 1, 1),
+            (cross, 0, 2), (cross, 2, 1), (relay, 1, 2), (cross, 0, 3), (cross, 2, 2), (start_kv, 0),
         ],
     )
     ready(v0)
     up_step(v0, 0)
     at([(arrive, 1, 3), (cross, 1, 0)], [(relay, 1, 3), (cross, 2, 3), (start_kv, 1), (cross, 1, 0)])
     up_step(v0, 1)
-    at([(arrive, 2, 0), (cross, 1, 1)], [(cross, 1, 1)])
+    at([(arrive, 2, 0), (start_tables,), (cross, 1, 1)], [(cross, 1, 1)])
     up_step(v0, 2)
-    at([(arrive, 2, 1), (cross, 1, 2)], [(cross, 1, 2)])
+    at([(arrive, 2, 1), (cross, 1, 2)], [(cross, 1, 2), (pass_kv, 0)])
     down_far(v0)
     at([(arrive, 2, 2), (cross, 1, 3)], [(cross, 1, 3)])
     down_near(v0)
     own_sums()
-    at([(arrive, 2, 3)] + [(reduce_own, h, False) for h in early], [(reduce_core, v0)])
+    at([(arrive, 2, 3), (reduce_z_far, v0)], [(reduce_core, v0)])
     ready(v1)
     up_step(v1, 0)
-    at([(reduce_z, v0), (cross, 2, 0), (cross, 2, 1)], [(pass_kv, 2)])
+    at([(reduce_z_near, v0), (cross, 2, 0), (cross, 2, 1)], [(pass_kv, 2)])
     up_step(v1, 1)
     at([(cross, 2, 2)], [])
     up_step(v1, 2)
+    at([], [(weigh,)])
     down_far(v1)
-    at([(cross, 2, 3)], [(pass_kv, 0)])
+    at([(cross, 2, 3)], [(finish, 0, 0, ret_copy)])
     down_near(v1)
     reduce_core(v1)
-    at([], [(reduce_x, v0, h) for h in early])
+    at([(weigh,)], [(finish, 0, 1, ret_copy), (pass_kv, 1)])
     ready(v2)
     up_step(v2, 0)
-    at([], [(reduce_x, v0, 2)])
+    at([], [(finish, 0, 2, ret_copy)])
     up_step(v2, 1)
-    at([], [(pass_kv, 1)])
+    at([], [(finish, 0, 3, ret_copy)])
     up_step(v2, 2)
-    at([], [(reduce_x, v0, 3)])
     down_far(v2)
-    at([(reduce_x, v1, 0)], [])
     down_near(v2)
     reduce_core(v2)
-    reduce_rest = [(reduce_x, v1, h) for h in early]
-    at(reduce_rest[1:], reduce_rest)
-    at([(take_kv, k) for k in range(n - 1)], [])
-    attend(0)
-    reduce_x(v1, 2)
-    for h in range(1, lam_ref.shape[0]):
-        attend(h)
-    reduce_x(v1, 3)
-
-    def settle(joined, hs):
-        waiter(s_out.at[v2], r2_send.at[v2], r2_recv.at[v2, 0]).wait_send()
-        for h in hs:
-            reduce_own(h, joined)
-        for h in halves:
-            reduce_x(v2, h)
-
-    at([(settle, False, late)], [(settle, True, halves)])
+    at([(finish, 1, h, join_copy) for h in halves], [(finish, 1, h, ret_copy) for h in halves])
+
+    def attention():
+        for k in range(n - 1):
+            take_kv(k)
+        for h in range(lam_ref.shape[0]):
+            attend(h)
+
+    def attention_here():
+        for h in range(lam_ref.shape[0]):
+            attend(h)
+
+    at(
+        [(finish, 2, h, ret_copy) for h in early] + [(drained, 2)]
+        + [(reduce_own, h, False) for h in halves] + [(finish, 2, h, ret_copy) for h in late]
+        + [(attention,)],
+        [(finish, 2, h, ret_copy, True) for h in early] + [(drained, 2), (take_zo,)]
+        + [(reduce_own, h, True) for h in halves]
+        + [(finish, 2, h, ret_copy, True) for h in late] + [(attention_here,)],
+    )
 
     for h in halves:
         r2_copy(e, h).wait_recv()
@@ -601,16 +642,17 @@
 
     def gather_back(ks):
         for k in ks:
+            waiter(ret.at[visits[k]], r3_send.at[0], r3_recv.at[visits[k]]).wait_recv()
             for h in halves:
                 add_back(k, h, k == ks[-1])
 
     @on_outer
     def _():
-        gather_back((1, 0, 2))
+        gather_back((0, 1, 2))
 
     @on_inner
     def _():
-        gather_back((0, 1))
+        gather_back((2,))
 
     def sent(ref, sem):
         waiter(ref, sem, c_recv.at[e]).wait_send()
@@ -620,14 +662,16 @@
     sent(gathered.at[pl.ds(0, 3), :, double], c_send.at[0])
     sent(gathered.at[pl.ds(0, 2), :, quarter], own_send.at[0])
     sent(s_out.at[e], r2_send.at[e])
+    sent(tables.at[pl.ds(0, 3)], tab_send.at[0])
     sent(s_out.at[v1], r2_send.at[v1])
 
     @on_outer
     def _():
-        sent(kv.at[pl.ds(0, kv_rows)], kv_own_send.at[0])
         sent(gathered.at[pl.ds(0, 3), :, quarter], x_send.at[0])
         sent(z_out, zo_send.at[0])
-        sent(t_out.at[pl.ds(0, 2)], r3_send.at[0])
+        sent(kv.at[pl.ds(0, kv_rows)], kv_own_send.at[0])
+        sent(t_out.at[0], r3_send.at[0])
+        sent(t_out.at[0], join_send.at[0])
 
     @on_inner
     def _():
@@ -683,9 +727,13 @@
             pltpu.VMEM((n, rows, cols), BF16),
             pltpu.VMEM((2, rows, cols), BF16),
             pltpu.VMEM((2, rows, cols), BF16),
-            pltpu.VMEM((rows, -(-n // 8) * 8), F32),
+            pltpu.VMEM((rows, cols), BF16),
+            pltpu.VMEM((-(-n // 8) * 8, rows), F32),
+            pltpu.VMEM((n, -(-n // 8) * 8, rows), F32),
+            pltpu.VMEM((rows, 8), F32),
+            pltpu.VMEM((rows, 8), F32),
             dma((3,)),
-            dma((1,)),
+            dma((PIECES,)),
             dma((8,)),
             dma((1,)),
             dma((1,)),
@@ -702,9 +750,13 @@
             dma((n,)),
             dma((n, PIECES)),
             dma((1,)),
-            dma((n, PIECES)),
-            dma((1,)),
-            dma((2, PIECES)),
+            dma((n,)),
+            dma((1,)),
+            dma((1,)),
+            dma((1,)),
+            dma((PIECES,)),
+            dma((1,)),
+            dma((n,)),
         ],
         compiler_params=pltpu.CompilerParams(
             collective_id=0, has_side_effects=True, vmem_limit_bytes=60 * 1024 * 1024

time: 49.3 us -> 44.2 us (0.90)
  the two profiles are of different devices: /device:TPU:0 before, /device:TPU:9 now
where the time goes in v2:
time: 44.2 us; the launch traced here: 44.1 us
  Pallas kernels  43.4 us (98%)
  between operations  0.64 us (1%)
    pallas_call x1, Pallas kernels, fused(): pl.pallas_call(functools.partial(fused_kernel, n), out_shape=(pltpu.VMEM(...  42.7 us

profile of v2, /device:TPU:9, one launch (start us, length us, event | category | flops | bytes accessed | tf_op | source)
XLA Modules:
  0.0 44.1 jit_solution(10911208325191832078)
XLA Ops:
  0.6 42.7 %fused_layer.1 = (bf16[128,256]{1,0:T(8,128)(2,1)S(1)}, bf16[256,384]{1,0:T(8,128)(2,1)S(1)}) custom-call(bf16[128,256]{1,0:T(8,128)(2,1)} %q_hbm.1, bf16[128,256]{1,0:T(8,128)(2,1)} %k_hbm.1, bf16[128,256]{1,0:T(8,128)(2,1)} %v_hbm.1, f32[2]{0:T(128)} %lam_hbm.1, f32[128]{0:T(128)} %hgain_hbm.1, bf16[256,1536]{1,0:T(8,128)(2,1)} %tok_hbm.1, ...), custom_call_target="tpu_custom_call" | custom-call | tf_op jit(solution)/shard_map/fused_layer/pallas_call | solution.py:699
  43.3 0.7 %hand_on.1 = (bf16[128,256]{1,0:T(8,128)(2,1)}, bf16[256,384]{1,0:T(8,128)(2,1)}) custom-call(bf16[128,256]{1,0:T(8,128)(2,1)S(1)} %get-tuple-element.4.a_ref, bf16[256,384]{1,0:T(8,128)(2,1)S(1)} %get-tuple-element.5.b_ref), custom_call_target="tpu_custom_call" | custom-call | tf_op jit(solution)/shard_map/hand_on/pallas_call | solution.py:779

commit v3 on v2

--- a/solution.py
+++ b/solution.py
@@ -371,11 +371,11 @@
     def along(s, h):
         return part[s, half(h), colblock(t)].astype(F32) + core_in[s, xi, half(h)].astype(F32)
 
-    def reduce_core(s):
-        r1_copy(s, 1 - xi).wait_recv()
-        for h in halves:
-            s_out[s, half(h)] = across(s, h).astype(BF16)
-            r2_copy(s, h).start()
+    def exchange(s, h):
+        if h == 0:
+            r1_copy(s, 1 - xi).wait_recv()
+        s_out[s, half(h)] = across(s, h).astype(BF16)
+        r2_copy(s, h).start()
 
     def reduce_z_far(s):
         r1_copy(s, 1 - xi).wait_recv()
@@ -593,29 +593,42 @@
     at([(arrive, 2, 2), (cross, 1, 3)], [(cross, 1, 3)])
     down_near(v0)
     own_sums()
-    at([(arrive, 2, 3), (reduce_z_far, v0)], [(reduce_core, v0)])
+    at([(arrive, 2, 3), (reduce_z_far, v0)], [(exchange, v0, 0)])
     ready(v1)
     up_step(v1, 0)
-    at([(reduce_z_near, v0), (cross, 2, 0), (cross, 2, 1)], [(pass_kv, 2)])
+    at(
+        [(reduce_z_near, v0), (cross, 2, 0), (cross, 2, 1)],
+        [(exchange, v0, 1), (pass_kv, 2)],
+    )
     up_step(v1, 1)
-    at([(cross, 2, 2)], [])
+    at([(cross, 2, 2)], [(exchange, v0, 2)])
     up_step(v1, 2)
-    at([], [(weigh,)])
+    at([], [(exchange, v0, 3), (weigh,)])
     down_far(v1)
     at([(cross, 2, 3)], [(finish, 0, 0, ret_copy)])
     down_near(v1)
-    reduce_core(v1)
+    exchange(v1, 0)
     at([(weigh,)], [(finish, 0, 1, ret_copy), (pass_kv, 1)])
     ready(v2)
     up_step(v2, 0)
+    exchange(v1, 1)
     at([], [(finish, 0, 2, ret_copy)])
     up_step(v2, 1)
+    exchange(v1, 2)
+    up_step(v2, 2)
+    exchange(v1, 3)
     at([], [(finish, 0, 3, ret_copy)])
-    up_step(v2, 2)
     down_far(v2)
+    at([], [(finish, 1, 0, ret_copy)])
     down_near(v2)
-    reduce_core(v2)
-    at([(finish, 1, h, join_copy) for h in halves], [(finish, 1, h, ret_copy) for h in halves])
+    exchange(v2, 0)
+    for h in halves:
+        at(
+            [(finish, 1, h, join_copy)],
+            [(finish, 1, h, ret_copy)] if h else [],
+        )
+        if h + 1 < PIECES:
+            exchange(v2, h + 1)
 
     def attention():
         for k in range(n - 1):

time: 44.2 us -> 43.2 us (0.977)
  the two profiles are of different devices: /device:TPU:9 before, /device:TPU:0 now
where the time goes in v3:
time: 43.2 us; the launch traced here: 42.8 us
  Pallas kernels  42.2 us (98%)
  between operations  0.64 us (1%)
    pallas_call x1, Pallas kernels, fused(): pl.pallas_call(functools.partial(fused_kernel, n), out_shape=(pltpu.VMEM(...  41.5 us

profile of v3, /device:TPU:0, one launch (start us, length us, event | category | flops | bytes accessed | tf_op | source)
XLA Modules:
  0.0 42.8 jit_solution(8432551952844296594)
XLA Ops:
  0.6 41.5 %fused_layer.1 = (bf16[128,256]{1,0:T(8,128)(2,1)S(1)}, bf16[256,384]{1,0:T(8,128)(2,1)S(1)}) custom-call(bf16[128,256]{1,0:T(8,128)(2,1)} %q_hbm.1, bf16[128,256]{1,0:T(8,128)(2,1)} %k_hbm.1, bf16[128,256]{1,0:T(8,128)(2,1)} %v_hbm.1, f32[2]{0:T(128)} %lam_hbm.1, f32[128]{0:T(128)} %hgain_hbm.1, bf16[256,1536]{1,0:T(8,128)(2,1)} %tok_hbm.1, ...), custom_call_target="tpu_custom_call" | custom-call | tf_op jit(solution)/shard_map/fused_layer/pallas_call | solution.py:712
  42.1 0.7 %hand_on.1 = (bf16[128,256]{1,0:T(8,128)(2,1)}, bf16[256,384]{1,0:T(8,128)(2,1)}) custom-call(bf16[128,256]{1,0:T(8,128)(2,1)S(1)} %get-tuple-element.4.a_ref, bf16[256,384]{1,0:T(8,128)(2,1)S(1)} %get-tuple-element.5.b_ref), custom_call_target="tpu_custom_call" | custom-call | tf_op jit(solution)/shard_map/hand_on/pallas_call | solution.py:792

commit v4 on v3

--- a/solution.py
+++ b/solution.py
@@ -433,9 +433,8 @@
             tab_back(s).wait_recv()
         weights_at[...] = columns([line_of(tables[s], e) for s in visits])
 
-    def start_tables():
-        for s in visits:
-            tab_copy(s).start()
+    def start_table(k):
+        tab_copy(visits[k]).start()
 
     def arrive(k, h, x=True):
         z_copy(k, h).wait_recv()
@@ -574,11 +573,12 @@
     down_near(e)
     at(
         [
-            (arrive, 1, 0), (cross, 0, 1), (arrive, 1, 1), (cross, 0, 2), (arrive, 1, 2),
+            (arrive, 1, 0), (start_table, 0), (start_table, 1), (cross, 0, 1), (arrive, 1, 1),
+            (cross, 0, 2), (arrive, 1, 2),
             (cross, 0, 3),
         ],
         [
-            (relay, 1, 0), (start_tables,), (cross, 0, 1), (cross, 2, 0), (relay, 1, 1),
+            (relay, 1, 0), (start_table, 0), (start_table, 1), (start_table, 2), (cross, 0, 1), (cross, 2, 0), (relay, 1, 1),
             (cross, 0, 2), (cross, 2, 1), (relay, 1, 2), (cross, 0, 3), (cross, 2, 2), (start_kv, 0),
         ],
     )
@@ -586,35 +586,36 @@
     up_step(v0, 0)
     at([(arrive, 1, 3), (cross, 1, 0)], [(relay, 1, 3), (cross, 2, 3), (start_kv, 1), (cross, 1, 0)])
     up_step(v0, 1)
-    at([(arrive, 2, 0), (start_tables,), (cross, 1, 1)], [(cross, 1, 1)])
+    at([(arrive, 2, 0), (start_table, 2), (cross, 1, 1)], [(cross, 1, 1)])
     up_step(v0, 2)
     at([(arrive, 2, 1), (cross, 1, 2)], [(cross, 1, 2), (pass_kv, 0)])
     down_far(v0)
     at([(arrive, 2, 2), (cross, 1, 3)], [(cross, 1, 3)])
     down_near(v0)
     own_sums()
-    at([(arrive, 2, 3), (reduce_z_far, v0)], [(exchange, v0, 0)])
+    at([(arrive, 2, 3), (reduce_z_far, v0)], [(exchange, v0, 0), (pass_kv, 2), (weigh,)])
     ready(v1)
     up_step(v1, 0)
     at(
-        [(reduce_z_near, v0), (cross, 2, 0), (cross, 2, 1)],
-        [(exchange, v0, 1), (pass_kv, 2)],
+        [(reduce_z_near, v0), (cross, 2, 0)],
+        [(exchange, v0, 1)],
     )
     up_step(v1, 1)
-    at([(cross, 2, 2)], [(exchange, v0, 2)])
+    at([(cross, 2, 1)], [(exchange, v0, 2)])
     up_step(v1, 2)
-    at([], [(exchange, v0, 3), (weigh,)])
+    at([(cross, 2, 2)], [(exchange, v0, 3)])
     down_far(v1)
     at([(cross, 2, 3)], [(finish, 0, 0, ret_copy)])
     down_near(v1)
     exchange(v1, 0)
-    at([(weigh,)], [(finish, 0, 1, ret_copy), (pass_kv, 1)])
+    at([(weigh,)], [(pass_kv, 1)])
     ready(v2)
     up_step(v2, 0)
     exchange(v1, 1)
-    at([], [(finish, 0, 2, ret_copy)])
+    at([], [(finish, 0, 1, ret_copy)])
     up_step(v2, 1)
     exchange(v1, 2)
+    at([], [(finish, 0, 2, ret_copy)])
     up_step(v2, 2)
     exchange(v1, 3)
     at([], [(finish, 0, 3, ret_copy)])

time: 43.2 us -> 43 us (level)
  no operation moved by 1% of the time
where the time goes in v4:
time: 43 us; the launch traced here: 42.4 us
  Pallas kernels  41.8 us (97%)
  between operations  0.64 us (1%)
    pallas_call x1, Pallas kernels, fused(): pl.pallas_call(functools.partial(fused_kernel, n), out_shape=(pltpu.VMEM(...  41.1 us

profile of v4, /device:TPU:0, one launch (start us, length us, event | category | flops | bytes accessed | tf_op | source)
XLA Modules:
  0.0 42.4 jit_solution(219567849255427938)
XLA Ops:
  0.6 41.1 %fused_layer.1 = (bf16[128,256]{1,0:T(8,128)(2,1)S(1)}, bf16[256,384]{1,0:T(8,128)(2,1)S(1)}) custom-call(bf16[128,256]{1,0:T(8,128)(2,1)} %q_hbm.1, bf16[128,256]{1,0:T(8,128)(2,1)} %k_hbm.1, bf16[128,256]{1,0:T(8,128)(2,1)} %v_hbm.1, f32[2]{0:T(128)} %lam_hbm.1, f32[128]{0:T(128)} %hgain_hbm.1, bf16[256,1536]{1,0:T(8,128)(2,1)} %tok_hbm.1, ...), custom_call_target="tpu_custom_call" | custom-call | tf_op jit(solution)/shard_map/fused_layer/pallas_call | solution.py:713
  41.7 0.7 %hand_on.1 = (bf16[128,256]{1,0:T(8,128)(2,1)}, bf16[256,384]{1,0:T(8,128)(2,1)}) custom-call(bf16[128,256]{1,0:T(8,128)(2,1)S(1)} %get-tuple-element.4.a_ref, bf16[256,384]{1,0:T(8,128)(2,1)S(1)} %get-tuple-element.5.b_ref), custom_call_target="tpu_custom_call" | custom-call | tf_op jit(solution)/shard_map/hand_on/pallas_call | solution.py:793
